TPU v7x, 32 devices: a whole 2x2x4 slice. The times are simulated.
32 devices in a mesh: grp: 2 (over y), sp: 4 (over z), tp: 4 (over x, core).
Axes of the slice: x: 2, y: 2, z: 4, core: 2. Of those that a mesh axis runs over, the one named last changes fastest.
Arguments:
- layer_input: bfloat16 [8, 1536, 2048], P(('grp', 'tp'), 'sp'), parts along dimension 0, may hold values from -6 to 6
- input_gain: float32 [2048], replicated, may hold values from 0.1 to 1.9
- key_weight: bfloat16 [2048, 512], replicated, may hold values from -0.125 to 0.125
- value_weight: bfloat16 [2048, 512], replicated, may hold values from -0.125 to 0.125
- stick_offsets: bfloat16 [4, 8, 1536], P(None, ('grp', 'tp'), 'sp'), parts along dimension 1
- head_bias: float32 [16], replicated
- queries: bfloat16 [8, 4, 512], P(('grp', 'tp'), 'sp'), parts along dimension 0, may hold values from -6 to 6
Outputs:
- key_cache: bfloat16 [8, 4, 1536, 128], P(('grp', 'tp'), 'sp'), parts along dimension 0
- value_cache: bfloat16 [8, 4, 1536, 128], P(('grp', 'tp'), 'sp'), parts along dimension 0
- offset_cache: bfloat16 [8, 4, 1536], P(('grp', 'tp'), 'sp'), parts along dimension 0
- first_read: bfloat16 [8, 4, 512], P(('grp', 'tp'), 'sp'), parts along dimension 0
There are 2 independent parts, one for each index of `grp`. A program takes and returns all parts, laid end to end along the dimension named above; an argument that names none is the same for every part. Nothing has to cross between parts.
All inputs are finite; a program needn't handle non-finite values.
Results may differ from a plain program's by a relative error of at most 0.014.
Values may be sent and summed in bfloat16 or wider, within the bound.
A program may use at most 64 MiB of HBM per device.

v0:
```python
import math

import jax
import jax.numpy as jnp
from jax import lax
from jax.sharding import PartitionSpec as P

H = 16
KVH = 4
HD = 128


EPSILON = 1e-06


def rms_scale(matrix):
    return matrix * lax.rsqrt(jnp.mean(matrix * matrix, axis=-1, keepdims=True) + EPSILON)


def stick_weights(scores, spread, carried):
    inside = lax.cumsum(spread, axis=scores.ndim - 1, reverse=True) - spread
    return jnp.exp(jax.nn.log_sigmoid(scores) - inside - carried)


def normalize(rows, input_gain):
    return (rms_scale(rows.astype(jnp.float32)) * input_gain).astype(jnp.bfloat16)


def project(normed_rows, weight):
    return jnp.dot(normed_rows, weight, preferred_element_type=jnp.float32).astype(jnp.bfloat16)


def shards(layer_input, input_gain, key_weight, value_weight, stick_offsets, head_bias, queries):
    seq_count, block_len, model_width = layer_input.shape
    sp_count = lax.axis_size("sp")
    group_size = H // KVH
    length = sp_count * block_len
    offset_lookup_matrix = head_bias.reshape(KVH, group_size)
    offset_parts = jnp.transpose(stick_offsets, (1, 0, 2)).reshape(sp_count, block_len)
    head_index = lax.axis_index("sp") % KVH
    normed_rows = normalize(layer_input.reshape(seq_count * block_len, model_width), input_gain)
    key_rows = project(normed_rows, key_weight).reshape(seq_count, block_len, KVH, HD)
    value_rows = project(normed_rows, value_weight).reshape(seq_count, block_len, KVH, HD)
    key_rows, value_rows = (key_rows, value_rows)
    key_parts = jnp.transpose(key_rows, (0, 2, 1, 3)).reshape(sp_count, block_len, HD)
    value_parts = jnp.transpose(value_rows, (0, 2, 1, 3)).reshape(sp_count, block_len, HD)
    key_cache, value_cache, offset_cache = (
        lax.all_to_all(key_parts, "sp", split_axis=0, concat_axis=1, tiled=True),
        lax.all_to_all(value_parts, "sp", split_axis=0, concat_axis=1, tiled=True),
        lax.all_to_all(offset_parts, "sp", split_axis=0, concat_axis=1, tiled=True),
    )
    key_cache = key_cache.reshape(1, 1, length, HD)
    value_cache = value_cache.reshape(1, 1, length, HD)
    offset_cache = offset_cache.reshape(1, 1, length)
    bias_row = lax.dynamic_index_in_dim(offset_lookup_matrix, head_index, 0, keepdims=False)
    own_query = queries.reshape(group_size, HD)
    scores = lax.dot_general(
        own_query,
        key_cache.reshape(length, HD),
        (((1,), (1,)), ((), ())),
        preferred_element_type=jnp.float32,
    )
    scores = (
        scores / math.sqrt(HD)
        + bias_row[:, None]
        + offset_cache.reshape(1, length).astype(jnp.float32)
    )
    spread = jax.nn.softplus(scores)
    weights = stick_weights(scores, spread, 0.0).astype(jnp.bfloat16)
    mixture = jnp.dot(weights, value_cache.reshape(length, HD), preferred_element_type=jnp.float32)
    first_read = rms_scale(mixture).astype(jnp.bfloat16).reshape(1, 1, group_size * HD)
    return (key_cache, value_cache, offset_cache, first_read)


def solution(mesh):
    placed = (
        P(("grp", "tp"), "sp", None),
        P(),
        P(),
        P(),
        P(None, ("grp", "tp"), "sp"),
        P(),
        P(("grp", "tp"), "sp", None),
    )
    return jax.shard_map(
        shards,
        mesh=mesh,
        in_specs=placed,
        out_specs=(
            P(("grp", "tp"), "sp", None, None),
            P(("grp", "tp"), "sp", None, None),
            P(("grp", "tp"), "sp", None),
            P(("grp", "tp"), "sp", None),
        ),
        check_vma=False,
    )
```

profile of v0, /device:TPU:0, one launch (start us, length us, event | category | flops | bytes accessed | tf_op | source)
XLA Modules:
  0.0 48.2 jit_solution(10300464463350270427)
XLA Ops:
  0.6 0.0 copy-start
  0.6 0.5 %broadcast.48 = bf16[]{:T(256)} broadcast(bf16[]{:T(256)} %constant.45), dimensions={} | broadcast | bytes 4 | tf_op args[4]
  1.2 1.5 %reduce.5 = bf16[4,384]{1,0:T(4,128)(2,1)S(1)} reduce(bf16[4,1,384]{2,0,1:T(4,128)(2,1)} %param.11, bf16[]{:T(256)} %broadcast.48), dimensions={1}, to_apply=%copy.20.reduce_sub_computation | reduce | bytes 6146 | tf_op args[4]
  2.6 0.7 %reshape.118 = bf16[4,2,192]{2,1,0:T(2,128)(2,1)} reshape(bf16[4,384]{1,0:T(4,128)(2,1)S(1)} %reduce.5) | data formatting | bytes 6144
  3.3 6.3 %all-to-all-start.2 = ((bf16[4,2,192]{2,1,0:T(2,128)(2,1)}), bf16[4,2,192]{2,1,0:T(2,128)(2,1)S(1)}, u32[]{:S(2)}, u32[]{:S(2)}) async-start(bf16[4,2,192]{2,1,0:T(2,128)(2,1)} %reshape.118), calls=%async_computation.2 | async-start | bytes 8192 | tf_op jit(solution)/shard_map/all_to_all | solution.py:50
  9.6 1.8 %fusion = f32[384]{0:T(512)S(1)} fusion(bf16[1,384,2048]{2,1,0:T(8,128)(2,1)} %param.7), kind=kLoop, calls=%fused_computation.2 | loop fusion | flops 2358912 | bytes 1574400 | tf_op jit(solution)/shard_map/reduce_sum | solution.py:17
  11.4 0.0 copy-done
  11.4 2.4 %convolution_convert_fusion.1 = bf16[384,512]{1,0:T(8,128)(2,1)S(1)} fusion(bf16[2048,512]{1,0:T(8,128)(2,1)S(1)} %copy-done, bf16[1,384,2048]{2,1,0:T(8,128)(2,1)} %param.7, f32[2048]{0:T(1024)} %param.8, f32[384]{0:T(512)S(1)} %add_rsqrt_fusion), kind=kOutput, calls=%fused_computation.10 | convolution fusion | flops 808648704 | bytes 4072960 | tf_op jit(solution)/shard_map/dot_general | solution.py:30
  13.9 0.0 copy-start.2
  13.9 0.0 copy-start.3
  13.9 0.0 copy-start.4
  13.9 0.1 reshape.101
  14.0 0.8 %copy.29 = bf16[1,384,4,128]{3,1,2,0:T(8,128)(2,1)} copy(bf16[1,384,4,128]{3,2,1,0:T(4,128)(2,1)S(1)} %reshape.101) | data formatting | bytes 786432 | tf_op jit(solution)/shard_map/reshape | solution.py:42
  14.8 0.4 all-to-all-done.2
  15.2 4.7 %all-to-all-start = ((bf16[4,384,128]{2,1,0:T(8,128)(2,1)}), bf16[4,384,128]{2,1,0:T(8,128)(2,1)S(1)}, u32[]{:S(2)}, u32[]{:S(2)}) async-start(bf16[4,384,128]{2,1,0:T(8,128)(2,1)} %bitcast.42), calls=%async_computation | async-start | bytes 786432 | tf_op jit(solution)/shard_map/all_to_all | solution.py:48
  19.9 0.0 copy-done.2
  19.9 0.0 copy-done.3
  19.9 0.1 reshape.109
  20.0 0.0 copy-done.4
  20.0 3.1 %convolution_convert_fusion = bf16[384,512]{1,0:T(8,128)(2,1)S(1)} fusion(bf16[2048,512]{1,0:T(8,128)(2,1)} %param.10, bf16[1,384,2048]{2,1,0:T(8,128)(2,1)} %param.7, f32[2048]{0:T(1024)S(1)} %copy-done.4, f32[384]{0:T(512)S(1)} %add_rsqrt_fusion), kind=kOutput, calls=%fused_computation.9 | convolution fusion | flops 808648704 | bytes 4072960 | tf_op jit(solution)/shard_map/dot_general | solution.py:30
  23.1 0.1 reshape.104
  23.2 0.8 %copy.28 = bf16[1,384,4,128]{3,1,2,0:T(8,128)(2,1)} copy(bf16[1,384,4,128]{3,2,1,0:T(4,128)(2,1)S(1)} %reshape.104) | data formatting | bytes 786432 | tf_op jit(solution)/shard_map/reshape | solution.py:43
  24.0 0.1 reshape.119
  24.1 0.0 copy-start.1
  24.1 6.9 %all-to-all-done = bf16[4,384,128]{2,1,0:T(8,128)(2,1)S(1)} async-done(((bf16[4,384,128]{2,1,0:T(8,128)(2,1)}), bf16[4,384,128]{2,1,0:T(8,128)(2,1)S(1)}, u32[]{:S(2)}, u32[]{:S(2)}) %all-to-all-start) | async-done | bytes 393248 | tf_op jit(solution)/shard_map/all_to_all | solution.py:48
  31.0 3.5 %all-to-all-start.1 = ((bf16[4,384,128]{2,1,0:T(8,128)(2,1)}), bf16[4,384,128]{2,1,0:T(8,128)(2,1)S(1)}, u32[]{:S(2)}, u32[]{:S(2)}) async-start(bf16[4,384,128]{2,1,0:T(8,128)(2,1)} %bitcast.41), calls=%async_computation.1 | async-start | bytes 786432 | tf_op jit(solution)/shard_map/all_to_all | solution.py:49
  34.6 0.2 compare_select_fusion
  34.8 5.0 %reduce-window.6 = f32[4,12,128]{2,1,0:T(8,128)S(1)} reduce-window(f32[4,12,128]{2,1,0:T(8,128)S(1)} %reshape.110, f32[]{:T(128)} %constant.32.clone.1), window={size=1x1x128 pad=0_0x0_0x0_127}, to_apply=%region_1.2 | reduce-window | flops 780288 | bytes 49156 | tf_op jit(solution)/shard_map/reduce-window
  39.8 0.1 slice_reduce_fusion
  39.9 0.2 reduce-window.9
  40.1 0.1 slice.7
  40.2 0.1 add_bitcast_fusion
  40.2 5.5 %all-to-all-done.1 = bf16[4,384,128]{2,1,0:T(8,128)(2,1)S(1)} async-done(((bf16[4,384,128]{2,1,0:T(8,128)(2,1)}), bf16[4,384,128]{2,1,0:T(8,128)(2,1)S(1)}, u32[]{:S(2)}, u32[]{:S(2)}) %all-to-all-start.1) | async-done | bytes 393248 | tf_op jit(solution)/shard_map/all_to_all | solution.py:49
  45.7 0.3 multiply_reduce_fusion
  46.0 0.1 multiply_convert_fusion
  46.1 0.6 %reshape.112 = bf16[1,1,512]{2,1,0:T(2,128)(2,1)} reshape(bf16[4,128]{1,0:T(4,128)(2,1)S(1)} %multiply_convert_fusion) | data formatting | bytes 2048 | tf_op jit(solution)/shard_map/reshape | solution.py:71
  46.7 0.7 %copy.33 = bf16[1,1,1536,128]{3,2,1,0:T(8,128)(2,1)} copy(bf16[1,1,1536,128]{3,2,1,0:T(8,128)(2,1)S(1)} %bitcast.44) | data formatting | bytes 786432
  47.5 0.7 %copy.34 = bf16[1,1,1536,128]{3,2,1,0:T(8,128)(2,1)} copy(bf16[1,1,1536,128]{3,2,1,0:T(8,128)(2,1)S(1)} %bitcast.46) | data formatting | bytes 786432
  48.2 0.0 copy-done.1
  (7 shorter events, 0.1 us)
Async XLA Ops:
  0.6 10.8 %copy-start = (bf16[2048,512]{1,0:T(8,128)(2,1)S(1)}, bf16[2048,512]{1,0:T(8,128)(2,1)}, u32[]{:S(2)}) copy-start(bf16[2048,512]{1,0:T(8,128)(2,1)} %param.9) | copy-start | bytes 6291460
  3.3 11.9 %all-to-all-start.2 = ((bf16[4,2,192]{2,1,0:T(2,128)(2,1)}), bf16[4,2,192]{2,1,0:T(2,128)(2,1)S(1)}, u32[]{:S(2)}, u32[]{:S(2)}) async-start(bf16[4,2,192]{2,1,0:T(2,128)(2,1)} %reshape.118), calls=%async_computation.2 | async-start | bytes 8192 | tf_op jit(solution)/shard_map/all_to_all | solution.py:50
  13.9 6.0 %copy-start.2 = (bf16[1,1,512]{2,1,0:T(2,128)(2,1)S(1)}, bf16[1,1,512]{2,1,0:T(2,128)(2,1)}, u32[]{:S(2)}) copy-start(bf16[1,1,512]{2,1,0:T(2,128)(2,1)} %param.13) | copy-start | bytes 3076
  13.9 6.0 %copy-start.3 = (f32[16]{0:T(128)S(1)}, f32[16]{0:T(128)}, u32[]{:S(2)}) copy-start(f32[16]{0:T(128)} %param.12) | copy-start | bytes 196
  13.9 6.1 %copy-start.4 = (f32[2048]{0:T(1024)S(1)}, f32[2048]{0:T(1024)}, u32[]{:S(2)}) copy-start(f32[2048]{0:T(1024)} %param.8) | copy-start | bytes 24580
  15.2 15.8 %all-to-all-start = ((bf16[4,384,128]{2,1,0:T(8,128)(2,1)}), bf16[4,384,128]{2,1,0:T(8,128)(2,1)S(1)}, u32[]{:S(2)}, u32[]{:S(2)}) async-start(bf16[4,384,128]{2,1,0:T(8,128)(2,1)} %bitcast.42), calls=%async_computation | async-start | bytes 786432 | tf_op jit(solution)/shard_map/all_to_all | solution.py:48
  24.1 24.1 %copy-start.1 = (bf16[4,1,384]{2,1,0:T(2,128)(2,1)}, bf16[4,1,384]{2,1,0:T(2,128)(2,1)S(1)}, u32[]{:S(2)}) copy-start(bf16[4,1,384]{2,1,0:T(2,128)(2,1)S(1)} %reshape.119) | copy-start | bytes 9220
  31.0 14.7 %all-to-all-start.1 = ((bf16[4,384,128]{2,1,0:T(8,128)(2,1)}), bf16[4,384,128]{2,1,0:T(8,128)(2,1)S(1)}, u32[]{:S(2)}, u32[]{:S(2)}) async-start(bf16[4,384,128]{2,1,0:T(8,128)(2,1)} %bitcast.41), calls=%async_computation.1 | async-start | bytes 786432 | tf_op jit(solution)/shard_map/all_to_all | solution.py:49
where the time goes:
time: 48.6 us; the launch traced here: 48.2 us
  starting transfers between devices  14.5 us (30%)
  waiting for transfers between devices  12.8 us (26%)
  other arithmetic  8.63 us (18%)
  matrix products  6.07 us (12%)
  local copies, waits for them, and re-layouts  5.47 us (11%)
  between operations  0.75 us (2%)
    all_to_all x1, waiting for transfers between devices, shards(): lax.all_to_all(key_parts, 'sp', split_axis=0, concat_axis=1, tiled=True)  6.92 us
    all_to_all x1, starting transfers between devices, shards(): lax.all_to_all(offset_parts, 'sp', split_axis=0, concat_axis=1, tiled=True)  6.35 us
    dot_general x2, matrix products, project(): jnp.dot(normed_rows, weight, preferred_element_type=jnp.float32)  5.52 us
    all_to_all x1, waiting for transfers between devices, shards(): lax.all_to_all(value_parts, 'sp', split_axis=0, concat_axis=1, tiled=True)  5.48 us
    another operation x2, other arithmetic  5.17 us
    all_to_all x1, starting transfers between devices, shards(): lax.all_to_all(key_parts, 'sp', split_axis=0, concat_axis=1, tiled=True)  4.7 us
    all_to_all x1, starting transfers between devices, shards(): lax.all_to_all(value_parts, 'sp', split_axis=0, concat_axis=1, tiled=True)  3.46 us
    unnamed x15, local copies, waits for them, and re-layouts  2.8 us
  transfers between devices with their start and end apart: 3, of which 3 were waited for; matrix products, arithmetic and copies ran while one was open for 31% of the time, Pallas kernels for 0%

commit v1 on v0

v1 whole, which is shorter than its diff:
```python
import functools
import math

import jax
import jax.numpy as jnp
from jax import lax
from jax.experimental import pallas as pl
from jax.experimental.pallas import tpu as pltpu
from jax.sharding import PartitionSpec as P

H = 16
KVH = 4
HD = 128
EPSILON = 1e-06
ROWS = 128
VMEM_BYTES = 67043328
SPARE_BYTES = 262144
MESH = pl.DeviceIdType.MESH


def ring_order(count):
    return sorted(range(1, count), key=lambda d: (min(d, count - d), d))


def kernel(
    n, seqs, x_hbm, gain_ref, wk_hbm, wv_hbm, off_hbm, bias_ref, q_hbm,
    k_land, v_land, off_out, read_out,
    x_buf, normed, weights, sends, off_in, off_send, off_land, q_buf, stick,
    x_sem, w_sem, small_sem, k_sem, v_sem, o_sem,
):
    total, width = x_buf.shape
    block = total // seqs
    length = n * block
    group = H // KVH
    me = lax.axis_index("sp")
    order = ring_order(n)
    head_order = []
    for d in order + [0]:
        if d % KVH not in head_order:
            head_order.append(d % KVH)

    def peer(d):
        return lax.rem(me + d, n)

    def source(d):
        return lax.rem(me + n - d, n)

    x_copies = []
    for c in range(total // ROWS):
        part = pl.ds(c * ROWS, ROWS)
        x_copies.append(pltpu.make_async_copy(x_hbm.at[part], x_buf.at[part], x_sem.at[c]))
        x_copies[-1].start()
    w_copies = {}
    for kind, w_hbm in enumerate((wk_hbm, wv_hbm)):
        for j in head_order:
            col = pl.multiple_of(lax.rem(me + j, KVH) * HD, HD)
            copy = pltpu.make_async_copy(
                w_hbm.at[:, pl.ds(col, HD)], weights.at[kind, j], w_sem.at[kind, j]
            )
            copy.start()
            w_copies[kind, j] = copy
    off_copy = pltpu.make_async_copy(off_hbm, off_in, small_sem.at[0])
    off_copy.start()
    q_copy = pltpu.make_async_copy(q_hbm, q_buf, small_sem.at[1])
    q_copy.start()

    barrier = pltpu.get_barrier_semaphore()
    for d in order:
        pl.semaphore_signal(barrier, inc=1, device_id={"sp": peer(d)}, device_id_type=MESH)

    gain = gain_ref[...]
    step_rows = 16
    for c in range(total // ROWS):
        x_copies[c].wait()

        def norm_step(i, _, c=c):
            rows = pl.ds(pl.multiple_of(c * ROWS + i * step_rows, step_rows), step_rows)
            x = x_buf[rows, :].astype(jnp.float32)
            scale = lax.rsqrt(jnp.mean(x * x, axis=-1, keepdims=True) + EPSILON)
            normed[rows, :] = (x * scale * gain).astype(jnp.bfloat16)
            return 0

        lax.fori_loop(0, ROWS // step_rows, norm_step, 0, unroll=4)

    waited = set()

    def project(kind, d, dst):
        j = d % KVH
        if (kind, j) not in waited:
            w_copies[kind, j].wait()
            waited.add((kind, j))
        base = 0 if seqs == 1 else lax.div(peer(d), KVH) * block
        if seqs == 1:
            rows = normed[...]
        else:
            rows = normed[pl.ds(pl.multiple_of(base, 16), block), :]
        dst[...] = jnp.dot(rows, weights[kind, j], preferred_element_type=jnp.float32).astype(jnp.bfloat16)

    def send(src, dst, sem, slot, d):
        copy = pltpu.make_async_remote_copy(
            src_ref=src, dst_ref=dst, send_sem=sem.at[0, slot], recv_sem=sem.at[1, slot],
            device_id={"sp": peer(d)}, device_id_type=MESH,
        )
        copy.start()
        return copy

    here = pl.ds(pl.multiple_of(me * block, block), block)
    k_copies, v_copies, o_copies = {}, {}, {}
    for i, d in enumerate(order):
        project(0, d, sends.at[0, d])
        if i == 0:
            pl.semaphore_wait(barrier, n - 1)
        k_copies[d] = send(sends.at[0, d], k_land.at[0, 0, here], k_sem, d, d)
        if i == 0:
            off_copy.wait()
            for s in range(seqs):
                values = off_in[s].astype(jnp.float32)
                for h in range(KVH):
                    off_send[s * KVH + h] = values[h:h + 1, :]
            off_land[me] = off_send[me]
    for d in order:
        o_copies[d] = send(off_send.at[peer(d)], off_land.at[me], o_sem, d, d)
    project(0, 0, k_land.at[0, 0, here])
    for d in order:
        project(1, d, sends.at[1, d])
        v_copies[d] = send(sends.at[1, d], v_land.at[0, 0, here], v_sem, d, d)
    project(1, 0, v_land.at[0, 0, here])

    q_copy.wait()
    q_all = q_buf[0].astype(jnp.float32)
    q_rows = jnp.concatenate([q_all[:, g * HD:(g + 1) * HD] for g in range(group)] * 2, axis=0)
    q_rows = q_rows.astype(jnp.bfloat16)
    for d in order:
        o_copies[d].wait_recv()
    off_row = jnp.concatenate([off_land[i] for i in range(n)], axis=1)
    off_out[0] = off_row.astype(jnp.bfloat16)
    head = lax.rem(me, KVH)
    row_id = lax.broadcasted_iota(jnp.int32, (2 * group, 1), 0)
    bias = jnp.zeros((2 * group, 1), jnp.float32)
    for g in range(group):
        value = bias_ref[head * group + g]
        bias = jnp.where((row_id == g) | (row_id == g + group), value, bias)
    for d in order:
        k_copies[d].wait_recv()
    scores = lax.dot_general(
        q_rows, k_land[0, 0], (((1,), (1,)), ((), ())), preferred_element_type=jnp.float32
    )
    scores = scores / math.sqrt(HD) + bias + off_row
    tail = jnp.log1p(jnp.exp(-jnp.abs(scores)))
    spread = jnp.maximum(scores, 0.0) + tail
    log_sig = jnp.minimum(scores, 0.0) - tail
    chunks = length // HD
    cut = [spread[:, c * HD:(c + 1) * HD] for c in range(chunks)]
    stacked = jnp.concatenate(cut, axis=0)
    after = (
        lax.broadcasted_iota(jnp.int32, (HD, HD), 0) > lax.broadcasted_iota(jnp.int32, (HD, HD), 1)
    ).astype(jnp.float32)
    inner = jnp.dot(
        stacked, after, preferred_element_type=jnp.float32, precision=lax.Precision.HIGHEST
    )
    sums = jnp.sum(stacked, axis=1, keepdims=True)
    carried = jnp.zeros((2 * group, 1), jnp.float32)
    for c in reversed(range(chunks)):
        rows = slice(c * 2 * group, (c + 1) * 2 * group)
        beyond = inner[rows] + carried
        stick[:, c * HD:(c + 1) * HD] = jnp.exp(log_sig[:, c * HD:(c + 1) * HD] - beyond)
        carried = carried + sums[rows]

    mixture = jnp.zeros((2 * group, HD), jnp.float32)
    for d in [0] + order:
        if d:
            v_copies[d].wait_recv()
        part = pl.ds(pl.multiple_of(source(d) * block, block), block)
        mixture = mixture + jnp.dot(
            stick[:, part].astype(jnp.bfloat16), v_land[0, 0, part, :], preferred_element_type=jnp.float32
        )
    scale = lax.rsqrt(jnp.mean(mixture * mixture, axis=-1, keepdims=True) + EPSILON)
    read = mixture * scale
    read_out[0] = jnp.concatenate([read[g:g + 1] for g in range(group)], axis=1).astype(jnp.bfloat16)

    for d in order:
        k_copies[d].wait_send()
        v_copies[d].wait_send()
        o_copies[d].wait_send()


def shards(layer_input, input_gain, key_weight, value_weight, stick_offsets, head_bias, queries):
    seqs, block, width = layer_input.shape
    n = lax.axis_size("sp")
    length = n * block
    total = seqs * block
    hbm = pl.BlockSpec(memory_space=pltpu.HBM)
    vmem = pl.BlockSpec(memory_space=pltpu.VMEM)
    smem = pl.BlockSpec(memory_space=pltpu.SMEM)
    group_width = queries.shape[-1]
    return pl.pallas_call(
        functools.partial(kernel, n, seqs),
        out_shape=(
            jax.ShapeDtypeStruct((1, 1, length, HD), jnp.bfloat16),
            jax.ShapeDtypeStruct((1, 1, length, HD), jnp.bfloat16),
            jax.ShapeDtypeStruct((1, 1, length), jnp.bfloat16),
            jax.ShapeDtypeStruct((1, 1, group_width), jnp.bfloat16),
        ),
        in_specs=[hbm, vmem, hbm, hbm, hbm, smem, hbm],
        out_specs=(vmem, vmem, vmem, vmem),
        scratch_shapes=[
            pltpu.VMEM((total, width), jnp.bfloat16),
            pltpu.VMEM((total, width), jnp.bfloat16),
            pltpu.VMEM((2, KVH, width, HD), jnp.bfloat16),
            pltpu.VMEM((2, n, block, HD), jnp.bfloat16),
            pltpu.VMEM((seqs, KVH, block), jnp.bfloat16),
            pltpu.VMEM((n, 1, block), jnp.float32),
            pltpu.VMEM((n, 1, block), jnp.float32),
            pltpu.VMEM((1, 1, group_width), jnp.bfloat16),
            pltpu.VMEM((2 * (H // KVH), length), jnp.float32),
            pltpu.SemaphoreType.DMA((total // ROWS,)),
            pltpu.SemaphoreType.DMA((2, KVH)),
            pltpu.SemaphoreType.DMA((2,)),
            pltpu.SemaphoreType.DMA((2, n)),
            pltpu.SemaphoreType.DMA((2, n)),
            pltpu.SemaphoreType.DMA((2, n)),
        ],
        compiler_params=pltpu.CompilerParams(
            collective_id=0, has_side_effects=True, vmem_limit_bytes=VMEM_BYTES - 4 * length * HD - SPARE_BYTES
        ),
    )(
        layer_input.reshape(total, width),
        input_gain.reshape(1, width),
        key_weight,
        value_weight,
        jnp.transpose(stick_offsets, (1, 0, 2)),
        head_bias,
        queries,
    )


def solution(mesh):
    placed = (
        P(("grp", "tp"), "sp", None),
        P(),
        P(),
        P(),
        P(None, ("grp", "tp"), "sp"),
        P(),
        P(("grp", "tp"), "sp", None),
    )
    return jax.shard_map(
        shards,
        mesh=mesh,
        in_specs=placed,
        out_specs=(
            P(("grp", "tp"), "sp", None, None),
            P(("grp", "tp"), "sp", None, None),
            P(("grp", "tp"), "sp", None),
            P(("grp", "tp"), "sp", None),
        ),
        check_vma=False,
    )
```

time: 48.6 us -> 35.9 us (0.74)
  Pallas kernels: 0 us -> 28.9 us
  starting transfers between devices: 14.5 us -> 0 us
  waiting for transfers between devices: 12.8 us -> 0 us
  other arithmetic: 8.63 us -> 0 us
  matrix products: 6.07 us -> 0 us
  local copies, waits for them, and re-layouts: 5.47 us -> 6.06 us
    pallas_call x0 -> x1, Pallas kernels: none -> 28.9 us  [shards(): pl.pallas_call(functools.partial(kernel, n, seqs), out_shape=(jax.ShapeDt...]
    all_to_all x3 -> x0, starting transfers between devices: 14.5 us -> none  [the longest x1 6.35 us: shards(): lax.all_to_all(offset_parts, 'sp', split_axis=0, concat_axis=1, tiled=True)]
    all_to_all x3 -> x0, waiting for transfers between devices: 12.8 us -> none  [the longest x1 6.92 us: shards(): lax.all_to_all(key_parts, 'sp', split_axis=0, concat_axis=1, tiled=True)]
    dot_general x4 -> x0, matrix products: 6.07 us -> none  [the longest x2 5.52 us: project(): jnp.dot(normed_rows, weight, preferred_element_type=jnp.float32)]
    another operation x2 -> x0, other arithmetic: 5.17 us -> none
    unnamed x15 -> x4, local copies, waits for them, and re-layouts: 2.8 us -> 6.06 us
    reshape x7 -> x0, local copies, waits for them, and re-layouts: 2.49 us -> none  [the longest x2 0.89 us: shards(): project(normed_rows, value_weight).reshape(seq_count, block_len, KVH, HD)]
    reduce_sum x1 -> x0, other arithmetic: 1.79 us -> none  [rms_scale(): jnp.mean(matrix * matrix, axis=-1, keepdims=True) + EPSILON]
  transfers between devices with their start and end apart: 3 -> 0, of which waited for: 3 -> 0; matrix products, arithmetic and copies ran while one was open for 31% -> 0% of each run, Pallas kernels for 0% -> 0%
where the time goes in v1:
time: 35.9 us; the launch traced here: 35.6 us
  Pallas kernels  28.9 us (81%)
  local copies, waits for them, and re-layouts  6.06 us (17%)
  between operations  0.64 us (2%)
    pallas_call x1, Pallas kernels, shards(): pl.pallas_call(functools.partial(kernel, n, seqs), out_shape=(jax.ShapeDt...  28.9 us
    unnamed x4, local copies, waits for them, and re-layouts  6.06 us

profile of v1, /device:TPU:0, one launch (start us, length us, event | category | flops | bytes accessed | tf_op | source)
XLA Modules:
  0.0 35.6 jit_solution(1410213967247811518)
XLA Ops:
  0.6 28.9 %shard_map.102 = (bf16[1,1,1536,128]{3,2,1,0:T(8,128)(2,1)}, bf16[1,1,1536,128]{3,2,1,0:T(8,128)(2,1)}, bf16[1,1,1536]{2,1,0:T(2,128)(2,1)}, bf16[1,1,512]{2,1,0:T(2,128)(2,1)}) custom-call(bf16[384,2048]{1,0:T(8,128)(2,1)} %bitcast.3, f32[1,2048]{1,0:T(1,128)} %bitcast.4, bf16[2048,512]{1,0:T(8,128)(2,1)} %wk_hbm.1, bf16[2048,512]{1,0:T(8,128)(2,1)} %wv_hbm.1, ...), custom_call_target="tpu_custom_call" | custom-call | tf_op jit(solution)/shard_map/pallas_call | solution.py:196
  29.5 1.8 %copy.15 = bf16[1,1,1536,128]{3,2,1,0:T(8,128)(2,1)} copy(bf16[1,1,1536,128]{3,2,1,0:T(8,128)(2,1)} %get-tuple-element.8) | data formatting | bytes 786432
  31.3 1.8 %copy.16 = bf16[1,1,1536,128]{3,2,1,0:T(8,128)(2,1)} copy(bf16[1,1,1536,128]{3,2,1,0:T(8,128)(2,1)} %get-tuple-element.9) | data formatting | bytes 786432
  33.0 1.3 %copy.17 = bf16[1,1,1536]{2,1,0:T(2,128)(2,1)} copy(bf16[1,1,1536]{2,1,0:T(2,128)(2,1)} %get-tuple-element.10) | data formatting | bytes 6144
  34.3 1.2 %copy.18 = bf16[1,1,512]{2,1,0:T(2,128)(2,1)} copy(bf16[1,1,512]{2,1,0:T(2,128)(2,1)} %get-tuple-element.11) | data formatting | bytes 2048

commit v2 on v1

--- a/solution.py
+++ b/solution.py
@@ -15,6 +15,7 @@
 ROWS = 128
 VMEM_BYTES = 67043328
 SPARE_BYTES = 262144
+WRITE_BYTES = 1048576
 MESH = pl.DeviceIdType.MESH
 
 
@@ -184,6 +185,18 @@
         o_copies[d].wait_send()
 
 
+def write_out(*refs):
+    *refs, sem = refs
+    half = len(refs) // 2
+    copies = [
+        pltpu.make_async_copy(refs[i], refs[half + i], sem.at[i]) for i in range(half)
+    ]
+    for copy in copies:
+        copy.start()
+    for copy in copies:
+        copy.wait()
+
+
 def shards(layer_input, input_gain, key_weight, value_weight, stick_offsets, head_bias, queries):
     seqs, block, width = layer_input.shape
     n = lax.axis_size("sp")
@@ -193,14 +206,15 @@
     vmem = pl.BlockSpec(memory_space=pltpu.VMEM)
     smem = pl.BlockSpec(memory_space=pltpu.SMEM)
     group_width = queries.shape[-1]
-    return pl.pallas_call(
+    outs = (
+        ((1, 1, length, HD), jnp.bfloat16),
+        ((1, 1, length, HD), jnp.bfloat16),
+        ((1, 1, length), jnp.bfloat16),
+        ((1, 1, group_width), jnp.bfloat16),
+    )
+    held = pl.pallas_call(
         functools.partial(kernel, n, seqs),
-        out_shape=(
-            jax.ShapeDtypeStruct((1, 1, length, HD), jnp.bfloat16),
-            jax.ShapeDtypeStruct((1, 1, length, HD), jnp.bfloat16),
-            jax.ShapeDtypeStruct((1, 1, length), jnp.bfloat16),
-            jax.ShapeDtypeStruct((1, 1, group_width), jnp.bfloat16),
-        ),
+        out_shape=tuple(pltpu.VMEM(*out) for out in outs),
         in_specs=[hbm, vmem, hbm, hbm, hbm, smem, hbm],
         out_specs=(vmem, vmem, vmem, vmem),
         scratch_shapes=[
@@ -232,6 +246,14 @@
         head_bias,
         queries,
     )
+    return pl.pallas_call(
+        write_out,
+        out_shape=tuple(jax.ShapeDtypeStruct(*out) for out in outs),
+        in_specs=[vmem] * len(outs),
+        out_specs=(hbm,) * len(outs),
+        scratch_shapes=[pltpu.SemaphoreType.DMA((len(outs),))],
+        compiler_params=pltpu.CompilerParams(vmem_limit_bytes=WRITE_BYTES),
+    )(*held)
 
 
 def solution(mesh):

time: 35.9 us -> 29.7 us (0.83)
  local copies, waits for them, and re-layouts: 6.06 us -> 0 us
    unnamed x4 -> x0, local copies, waits for them, and re-layouts: 6.06 us -> none
    pallas_call x1 -> x2, Pallas kernels: 28.9 us -> 28.9 us  [the longest x1 28 us: shards(): pl.pallas_call(functools.partial(kernel, n, seqs), out_shape=tuple((pltpu...]
where the time goes in v2:
time: 29.7 us; the launch traced here: 29.5 us
  Pallas kernels  28.9 us (97%)
  between operations  0.64 us (2%)
    pallas_call x1, Pallas kernels, shards(): pl.pallas_call(functools.partial(kernel, n, seqs), out_shape=tuple((pltpu...  28 us
    pallas_call x1, Pallas kernels, shards(): pl.pallas_call(write_out, out_shape=tuple((jax.ShapeDtypeStruct(*out) for...  0.92 us

profile of v2, /device:TPU:0, one launch (start us, length us, event | category | flops | bytes accessed | tf_op | source)
XLA Modules:
  0.0 29.5 jit_solution(9948454942711484677)
XLA Ops:
  0.6 28.0 %shard_map.102 = (bf16[1,1,1536,128]{3,2,1,0:T(8,128)(2,1)S(1)}, bf16[1,1,1536,128]{3,2,1,0:T(8,128)(2,1)S(1)}, bf16[1,1,1536]{2,1,0:T(2,128)(2,1)S(1)}, bf16[1,1,512]{2,1,0:T(2,128)(2,1)S(1)}) custom-call(bf16[384,2048]{1,0:T(8,128)(2,1)} %bitcast.3, f32[1,2048]{1,0:T(1,128)} %bitcast.4, bf16[2048,512]{1,0:T(8,128)(2,1)} %wk_hbm.1, ...), custom_call_target="tpu_custom_call" | custom-call | tf_op jit(solution)/shard_map/pallas_call | solution.py:215
  28.6 0.9 %shard_map.103 = (bf16[1,1,1536,128]{3,2,1,0:T(8,128)(2,1)}, bf16[1,1,1536,128]{3,2,1,0:T(8,128)(2,1)}, bf16[1,1,1536]{2,1,0:T(2,128)(2,1)}, bf16[1,1,512]{2,1,0:T(2,128)(2,1)}) custom-call(bf16[1,1,1536,128]{3,2,1,0:T(8,128)(2,1)S(1)} %get-tuple-element.8.refs_0_, bf16[1,1,1536,128]{3,2,1,0:T(8,128)(2,1)S(1)} %get-tuple-element.9.refs_1_, ...), custom_call_target="tpu_custom_call" | custom-call | tf_op jit(solution)/shard_map/pallas_call | solution.py:249

commit v3 on v2

--- a/solution.py
+++ b/solution.py
@@ -17,10 +17,6 @@
 SPARE_BYTES = 262144
 WRITE_BYTES = 1048576
 MESH = pl.DeviceIdType.MESH
-
-
-def ring_order(count):
-    return sorted(range(1, count), key=lambda d: (min(d, count - d), d))
 
 
 def kernel(
@@ -34,32 +30,44 @@
     length = n * block
     group = H // KVH
     me = lax.axis_index("sp")
-    order = ring_order(n)
-    head_order = []
-    for d in order + [0]:
-        if d % KVH not in head_order:
-            head_order.append(d % KVH)
-
-    def peer(d):
-        return lax.rem(me + d, n)
+    order = range(1, n)
+    paired = jnp.minimum(me, n - 1 - me)
+    toward = jnp.where(2 * me < n, 1, -1)
+
+    def peer(i):
+        near = me + toward * (1 if i % 2 else -1) * ((i + 1) // 2)
+        far = me + toward * (i - paired)
+        return jnp.where(i <= 2 * paired, near, far) if i else me
+
+    def offset(i):
+        return lax.rem(peer(i) - me + n, n)
 
     def source(d):
         return lax.rem(me + n - d, n)
+
+    first_head = lax.rem(peer(1), KVH)
+
+    def slot(i):
+        return lax.rem(lax.rem(peer(i), KVH) - first_head + KVH, KVH)
 
     x_copies = []
     for c in range(total // ROWS):
         part = pl.ds(c * ROWS, ROWS)
         x_copies.append(pltpu.make_async_copy(x_hbm.at[part], x_buf.at[part], x_sem.at[c]))
-        x_copies[-1].start()
     w_copies = {}
     for kind, w_hbm in enumerate((wk_hbm, wv_hbm)):
-        for j in head_order:
-            col = pl.multiple_of(lax.rem(me + j, KVH) * HD, HD)
-            copy = pltpu.make_async_copy(
+        for j in range(KVH):
+            col = pl.multiple_of(lax.rem(first_head + j, KVH) * HD, HD)
+            w_copies[kind, j] = pltpu.make_async_copy(
                 w_hbm.at[:, pl.ds(col, HD)], weights.at[kind, j], w_sem.at[kind, j]
             )
+    x_copies[0].start()
+    w_copies[0, 0].start()
+    for copy in x_copies[1:]:
+        copy.start()
+    for key, copy in w_copies.items():
+        if key != (0, 0):
             copy.start()
-            w_copies[kind, j] = copy
     off_copy = pltpu.make_async_copy(off_hbm, off_in, small_sem.at[0])
     off_copy.start()
     q_copy = pltpu.make_async_copy(q_hbm, q_buf, small_sem.at[1])
@@ -67,7 +75,7 @@
 
     barrier = pltpu.get_barrier_semaphore()
     for d in order:
-        pl.semaphore_signal(barrier, inc=1, device_id={"sp": peer(d)}, device_id_type=MESH)
+        pl.semaphore_signal(barrier, inc=1, device_id={"sp": source(d)}, device_id_type=MESH)
 
     gain = gain_ref[...]
     step_rows = 16
@@ -83,56 +91,69 @@
 
         lax.fori_loop(0, ROWS // step_rows, norm_step, 0, unroll=4)
 
-    waited = set()
-
-    def project(kind, d, dst):
-        j = d % KVH
-        if (kind, j) not in waited:
-            w_copies[kind, j].wait()
-            waited.add((kind, j))
-        base = 0 if seqs == 1 else lax.div(peer(d), KVH) * block
+    def project(kind, i, dst):
+        if i == 1:
+            w_copies[kind, 0].wait()
+        if i == 2:
+            for j in range(1, KVH):
+                w_copies[kind, j].wait()
         if seqs == 1:
             rows = normed[...]
         else:
+            base = lax.div(peer(i), KVH) * block
             rows = normed[pl.ds(pl.multiple_of(base, 16), block), :]
-        dst[...] = jnp.dot(rows, weights[kind, j], preferred_element_type=jnp.float32).astype(jnp.bfloat16)
-
-    def send(src, dst, sem, slot, d):
-        copy = pltpu.make_async_remote_copy(
-            src_ref=src, dst_ref=dst, send_sem=sem.at[0, slot], recv_sem=sem.at[1, slot],
-            device_id={"sp": peer(d)}, device_id_type=MESH,
+        dst[...] = jnp.dot(
+            rows, weights[kind, slot(i)], preferred_element_type=jnp.float32
+        ).astype(jnp.bfloat16)
+
+    def remote(src, dst, sem, d, target):
+        return pltpu.make_async_remote_copy(
+            src_ref=src, dst_ref=dst, send_sem=sem.at[0, d], recv_sem=sem.at[1, d],
+            device_id={"sp": target}, device_id_type=MESH,
         )
-        copy.start()
-        return copy
 
     here = pl.ds(pl.multiple_of(me * block, block), block)
-    k_copies, v_copies, o_copies = {}, {}, {}
-    for i, d in enumerate(order):
-        project(0, d, sends.at[0, d])
-        if i == 0:
+
+    def block_copy(kind, i):
+        land, sem = ((k_land, k_sem), (v_land, v_sem))[kind]
+        return remote(sends.at[kind, i], land.at[0, 0, here], sem, offset(i), peer(i))
+
+    def offset_copy(i):
+        return remote(off_send.at[peer(i)], off_land.at[me], o_sem, offset(i), peer(i))
+
+    for i in order:
+        project(0, i, sends.at[0, i])
+        if i == 1:
             pl.semaphore_wait(barrier, n - 1)
-        k_copies[d] = send(sends.at[0, d], k_land.at[0, 0, here], k_sem, d, d)
-        if i == 0:
+        block_copy(0, i).start()
+        if i == 1:
             off_copy.wait()
             for s in range(seqs):
                 values = off_in[s].astype(jnp.float32)
                 for h in range(KVH):
                     off_send[s * KVH + h] = values[h:h + 1, :]
             off_land[me] = off_send[me]
-    for d in order:
-        o_copies[d] = send(off_send.at[peer(d)], off_land.at[me], o_sem, d, d)
+    for i in order:
+        offset_copy(i).start()
+    for i in order:
+        project(1, i, sends.at[1, i])
+        block_copy(1, i).start()
     project(0, 0, k_land.at[0, 0, here])
-    for d in order:
-        project(1, d, sends.at[1, d])
-        v_copies[d] = send(sends.at[1, d], v_land.at[0, 0, here], v_sem, d, d)
     project(1, 0, v_land.at[0, 0, here])
+
+    def rows_of(i):
+        return pl.ds(pl.multiple_of(peer(i) * block, block), block)
+
+    def arrived(src, land, sem, i):
+        d = lax.rem(me - peer(i) + n, n)
+        remote(src, land.at[0, 0, rows_of(i)], sem, d, peer(i)).wait_recv()
 
     q_copy.wait()
     q_all = q_buf[0].astype(jnp.float32)
     q_rows = jnp.concatenate([q_all[:, g * HD:(g + 1) * HD] for g in range(group)] * 2, axis=0)
     q_rows = q_rows.astype(jnp.bfloat16)
     for d in order:
-        o_copies[d].wait_recv()
+        remote(off_send.at[0], off_land.at[source(d)], o_sem, d, source(d)).wait_recv()
     off_row = jnp.concatenate([off_land[i] for i in range(n)], axis=1)
     off_out[0] = off_row.astype(jnp.bfloat16)
     head = lax.rem(me, KVH)
@@ -142,7 +163,7 @@
         value = bias_ref[head * group + g]
         bias = jnp.where((row_id == g) | (row_id == g + group), value, bias)
     for d in order:
-        k_copies[d].wait_recv()
+        arrived(sends.at[0, d], k_land, k_sem, d)
     scores = lax.dot_general(
         q_rows, k_land[0, 0], (((1,), (1,)), ((), ())), preferred_element_type=jnp.float32
     )
@@ -168,10 +189,10 @@
         carried = carried + sums[rows]
 
     mixture = jnp.zeros((2 * group, HD), jnp.float32)
-    for d in [0] + order:
+    for d in range(n):
         if d:
-            v_copies[d].wait_recv()
-        part = pl.ds(pl.multiple_of(source(d) * block, block), block)
+            arrived(sends.at[1, d], v_land, v_sem, d)
+        part = rows_of(d)
         mixture = mixture + jnp.dot(
             stick[:, part].astype(jnp.bfloat16), v_land[0, 0, part, :], preferred_element_type=jnp.float32
         )
@@ -179,10 +200,10 @@
     read = mixture * scale
     read_out[0] = jnp.concatenate([read[g:g + 1] for g in range(group)], axis=1).astype(jnp.bfloat16)
 
-    for d in order:
-        k_copies[d].wait_send()
-        v_copies[d].wait_send()
-        o_copies[d].wait_send()
+    for i in order:
+        block_copy(0, i).wait_send()
+        block_copy(1, i).wait_send()
+        offset_copy(i).wait_send()
 
 
 def write_out(*refs):

time: 29.7 us -> 28.9 us (0.973)
  Pallas kernels: 28.9 us -> 28.1 us
    pallas_call x1, Pallas kernels: 28 us -> 27.1 us  [shards(): pl.pallas_call(functools.partial(kernel, n, seqs), out_shape=tuple((pltpu...]
where the time goes in v3:
time: 28.9 us; the launch traced here: 28.7 us
  Pallas kernels  28.1 us (97%)
  between operations  0.64 us (2%)
    pallas_call x1, Pallas kernels, shards(): pl.pallas_call(functools.partial(kernel, n, seqs), out_shape=tuple((pltpu...  27.1 us
    pallas_call x1, Pallas kernels, shards(): pl.pallas_call(write_out, out_shape=tuple((jax.ShapeDtypeStruct(*out) for...  0.92 us

profile of v3, /device:TPU:0, one launch (start us, length us, event | category | flops | bytes accessed | tf_op | source)
XLA Modules:
  0.0 28.7 jit_solution(268882028375043259)
XLA Ops:
  0.6 27.1 %shard_map.102 = (bf16[1,1,1536,128]{3,2,1,0:T(8,128)(2,1)S(1)}, bf16[1,1,1536,128]{3,2,1,0:T(8,128)(2,1)S(1)}, bf16[1,1,1536]{2,1,0:T(2,128)(2,1)S(1)}, bf16[1,1,512]{2,1,0:T(2,128)(2,1)S(1)}) custom-call(bf16[384,2048]{1,0:T(8,128)(2,1)} %bitcast.3, f32[1,2048]{1,0:T(1,128)} %bitcast.4, bf16[2048,512]{1,0:T(8,128)(2,1)} %wk_hbm.1, ...), custom_call_target="tpu_custom_call" | custom-call | tf_op jit(solution)/shard_map/pallas_call | solution.py:236
  27.8 0.9 %shard_map.103 = (bf16[1,1,1536,128]{3,2,1,0:T(8,128)(2,1)}, bf16[1,1,1536,128]{3,2,1,0:T(8,128)(2,1)}, bf16[1,1,1536]{2,1,0:T(2,128)(2,1)}, bf16[1,1,512]{2,1,0:T(2,128)(2,1)}) custom-call(bf16[1,1,1536,128]{3,2,1,0:T(8,128)(2,1)S(1)} %get-tuple-element.8.refs_0_, bf16[1,1,1536,128]{3,2,1,0:T(8,128)(2,1)S(1)} %get-tuple-element.9.refs_1_, ...), custom_call_target="tpu_custom_call" | custom-call | tf_op jit(solution)/shard_map/pallas_call | solution.py:270

commit v4 on v3

--- a/solution.py
+++ b/solution.py
@@ -13,6 +13,7 @@
 HD = 128
 EPSILON = 1e-06
 ROWS = 128
+PIECES = 4
 VMEM_BYTES = 67043328
 SPARE_BYTES = 262144
 WRITE_BYTES = 1048576
@@ -45,10 +46,8 @@
     def source(d):
         return lax.rem(me + n - d, n)
 
-    first_head = lax.rem(peer(1), KVH)
-
-    def slot(i):
-        return lax.rem(lax.rem(peer(i), KVH) - first_head + KVH, KVH)
+    def columns(i):
+        return pl.ds(pl.multiple_of(lax.rem(peer(i), KVH) * HD, HD), HD)
 
     x_copies = []
     for c in range(total // ROWS):
@@ -56,18 +55,18 @@
         x_copies.append(pltpu.make_async_copy(x_hbm.at[part], x_buf.at[part], x_sem.at[c]))
     w_copies = {}
     for kind, w_hbm in enumerate((wk_hbm, wv_hbm)):
-        for j in range(KVH):
-            col = pl.multiple_of(lax.rem(first_head + j, KVH) * HD, HD)
+        for j in range(PIECES):
+            part = pl.ds(j * (width // PIECES), width // PIECES)
             w_copies[kind, j] = pltpu.make_async_copy(
-                w_hbm.at[:, pl.ds(col, HD)], weights.at[kind, j], w_sem.at[kind, j]
+                w_hbm.at[part], weights.at[kind, part], w_sem.at[kind, j]
             )
     x_copies[0].start()
-    w_copies[0, 0].start()
+    for j in range(PIECES):
+        w_copies[0, j].start()
     for copy in x_copies[1:]:
         copy.start()
-    for key, copy in w_copies.items():
-        if key != (0, 0):
-            copy.start()
+    for j in range(PIECES):
+        w_copies[1, j].start()
     off_copy = pltpu.make_async_copy(off_hbm, off_in, small_sem.at[0])
     off_copy.start()
     q_copy = pltpu.make_async_copy(q_hbm, q_buf, small_sem.at[1])
@@ -79,10 +78,10 @@
 
     gain = gain_ref[...]
     step_rows = 16
-    for c in range(total // ROWS):
+    def norm(c):
         x_copies[c].wait()
 
-        def norm_step(i, _, c=c):
+        def norm_step(i, _):
             rows = pl.ds(pl.multiple_of(c * ROWS + i * step_rows, step_rows), step_rows)
             x = x_buf[rows, :].astype(jnp.float32)
             scale = lax.rsqrt(jnp.mean(x * x, axis=-1, keepdims=True) + EPSILON)
@@ -91,19 +90,20 @@
 
         lax.fori_loop(0, ROWS // step_rows, norm_step, 0, unroll=4)
 
+    def wait_weights(kind):
+        for j in range(PIECES):
+            w_copies[kind, j].wait()
+
     def project(kind, i, dst):
         if i == 1:
-            w_copies[kind, 0].wait()
-        if i == 2:
-            for j in range(1, KVH):
-                w_copies[kind, j].wait()
+            wait_weights(kind)
         if seqs == 1:
             rows = normed[...]
         else:
             base = lax.div(peer(i), KVH) * block
             rows = normed[pl.ds(pl.multiple_of(base, 16), block), :]
         dst[...] = jnp.dot(
-            rows, weights[kind, slot(i)], preferred_element_type=jnp.float32
+            rows, weights[kind, :, columns(i)], preferred_element_type=jnp.float32
         ).astype(jnp.bfloat16)
 
     def remote(src, dst, sem, d, target):
@@ -121,11 +121,30 @@
     def offset_copy(i):
         return remote(off_send.at[peer(i)], off_land.at[me], o_sem, offset(i), peer(i))
 
+    if seqs == 1:
+        for c in range(total // ROWS):
+            norm(c)
+            if c == 0:
+                wait_weights(0)
+            part = pl.ds(c * ROWS, ROWS)
+            sends[0, 1, part] = jnp.dot(
+                normed[part, :], weights[0, :, columns(1)], preferred_element_type=jnp.float32
+            ).astype(jnp.bfloat16)
+            if c == 0:
+                pl.semaphore_wait(barrier, n - 1)
+            there = pl.ds(pl.multiple_of(me * block + c * ROWS, ROWS), ROWS)
+            remote(
+                sends.at[0, 1, part], k_land.at[0, 0, there], k_sem, offset(1), peer(1)
+            ).start()
+    else:
+        for c in range(total // ROWS):
+            norm(c)
     for i in order:
-        project(0, i, sends.at[0, i])
-        if i == 1:
-            pl.semaphore_wait(barrier, n - 1)
-        block_copy(0, i).start()
+        if seqs > 1 or i > 1:
+            project(0, i, sends.at[0, i])
+            if i == 1:
+                pl.semaphore_wait(barrier, n - 1)
+            block_copy(0, i).start()
         if i == 1:
             off_copy.wait()
             for s in range(seqs):
@@ -241,7 +260,7 @@
         scratch_shapes=[
             pltpu.VMEM((total, width), jnp.bfloat16),
             pltpu.VMEM((total, width), jnp.bfloat16),
-            pltpu.VMEM((2, KVH, width, HD), jnp.bfloat16),
+            pltpu.VMEM((2, width, KVH * HD), jnp.bfloat16),
             pltpu.VMEM((2, n, block, HD), jnp.bfloat16),
             pltpu.VMEM((seqs, KVH, block), jnp.bfloat16),
             pltpu.VMEM((n, 1, block), jnp.float32),
@@ -249,7 +268,7 @@
             pltpu.VMEM((1, 1, group_width), jnp.bfloat16),
             pltpu.VMEM((2 * (H // KVH), length), jnp.float32),
             pltpu.SemaphoreType.DMA((total // ROWS,)),
-            pltpu.SemaphoreType.DMA((2, KVH)),
+            pltpu.SemaphoreType.DMA((2, PIECES)),
             pltpu.SemaphoreType.DMA((2,)),
             pltpu.SemaphoreType.DMA((2, n)),
             pltpu.SemaphoreType.DMA((2, n)),

time: 28.9 us -> 28.4 us (0.983)
  Pallas kernels: 28.1 us -> 27.5 us
    pallas_call x1, Pallas kernels: 27.1 us -> 26.6 us  [shards(): pl.pallas_call(functools.partial(kernel, n, seqs), out_shape=tuple((pltpu...]
where the time goes in v4:
time: 28.4 us; the launch traced here: 28.2 us
  Pallas kernels  27.5 us (97%)
  between operations  0.64 us (2%)
    pallas_call x1, Pallas kernels, shards(): pl.pallas_call(functools.partial(kernel, n, seqs), out_shape=tuple((pltpu...  26.6 us
    pallas_call x1, Pallas kernels, shards(): pl.pallas_call(write_out, out_shape=tuple((jax.ShapeDtypeStruct(*out) for...  0.92 us

profile of v4, /device:TPU:0, one launch (start us, length us, event | category | flops | bytes accessed | tf_op | source)
XLA Modules:
  0.0 28.2 jit_solution(15559168223507740681)
XLA Ops:
  0.6 26.6 %shard_map.102 = (bf16[1,1,1536,128]{3,2,1,0:T(8,128)(2,1)S(1)}, bf16[1,1,1536,128]{3,2,1,0:T(8,128)(2,1)S(1)}, bf16[1,1,1536]{2,1,0:T(2,128)(2,1)S(1)}, bf16[1,1,512]{2,1,0:T(2,128)(2,1)S(1)}) custom-call(bf16[384,2048]{1,0:T(8,128)(2,1)} %bitcast.3, f32[1,2048]{1,0:T(1,128)} %bitcast.4, bf16[2048,512]{1,0:T(8,128)(2,1)} %wk_hbm.1, ...), custom_call_target="tpu_custom_call" | custom-call | tf_op jit(solution)/shard_map/pallas_call | solution.py:255
  27.3 0.9 %shard_map.103 = (bf16[1,1,1536,128]{3,2,1,0:T(8,128)(2,1)}, bf16[1,1,1536,128]{3,2,1,0:T(8,128)(2,1)}, bf16[1,1,1536]{2,1,0:T(2,128)(2,1)}, bf16[1,1,512]{2,1,0:T(2,128)(2,1)}) custom-call(bf16[1,1,1536,128]{3,2,1,0:T(8,128)(2,1)S(1)} %get-tuple-element.8.refs_0_, bf16[1,1,1536,128]{3,2,1,0:T(8,128)(2,1)S(1)} %get-tuple-element.9.refs_1_, ...), custom_call_target="tpu_custom_call" | custom-call | tf_op jit(solution)/shard_map/pallas_call | solution.py:289
